TPU v7x, 32 devices: a whole 2x2x4 slice. The times are simulated.
32 devices in a mesh: rep: 2 (over x), fs: 8 (over z, y), tp: 2 (over core).
Axes of the slice: x: 2, y: 2, z: 4, core: 2. Of those that a mesh axis runs over, the one named last changes fastest.
Arguments:
- activations: bfloat16 [16384, 1024], P(('rep', 'fs', 'tp')), may hold values from -8 to 8
- mixer_gain: float32 [1024], replicated, may hold values from 0.1 to 1.9
- query_weight: bfloat16 [1024, 256], P('fs', 'tp'), may hold values from -0.1875 to 0.1875
- key_weight: bfloat16 [1024, 256], P('fs', 'tp'), may hold values from -0.1875 to 0.1875
- value_weight: bfloat16 [1024, 512], P('fs', 'tp'), may hold values from -0.1875 to 0.1875
- rank_weight: bfloat16 [1024, 16], replicated, may hold values from -0.1875 to 0.1875
- decay_gate_weight: bfloat16 [16, 256], P(None, 'tp'), may hold values from -1.5 to 1.5
- decay_gate_bias: float32 [256], P('tp'), may hold values from -1.5 to 8
- head_gain: float32 [256], replicated, may hold values from 0.1 to 1.9
- output_weight: bfloat16 [512, 1024], P('tp', 'fs'), may hold values from -0.25 to 0.25
- ffn_gain: float32 [1024], replicated, may hold values from 0.1 to 1.9
- gate_weight: bfloat16 [1024, 2816], P('fs', 'tp'), may hold values from -0.1875 to 0.1875
- up_weight: bfloat16 [1024, 2816], P('fs', 'tp'), may hold values from -0.1875 to 0.1875
- down_weight: bfloat16 [2816, 1024], P('tp', 'fs'), may hold values from -0.109375 to 0.109375
Outputs:
- result: bfloat16 [16384, 1024], P(('rep', 'fs', 'tp'))
All inputs are finite; a program needn't handle non-finite values.
Results may differ from a plain program's by a relative error of at most 0.0056.
Values may be sent and summed in bfloat16 or wider, within the bound.
No kernel may reach another device: no remote copies, remote signals or barrier semaphores. Data moves between devices by JAX's collectives and lax.ppermute only.
A program may use at most 64 MiB of HBM per device.

v0:
```python
import jax
import jax.numpy as jnp
from jax import lax
from jax.sharding import PartitionSpec as P

DK = 128
DV = 256
BLOCK = 64
epsilon = 1e-06
decay_softness = 16.0
highest = lax.Precision.HIGHEST


def rms_scale(values, gains):
    return values * lax.rsqrt(jnp.mean(values * values, axis=-1, keepdims=True) + epsilon) * gains


def linear_attention(queries, keys_all, values_all, decay_logarithm, head_count):
    length = queries.shape[0]
    number = length // BLOCK
    halfway = BLOCK // 2
    causal = jnp.tril(jnp.ones((BLOCK, BLOCK), bool))

    def to_blocks(matrix):
        return matrix.astype(jnp.float32).reshape(
            number, BLOCK, head_count, matrix.shape[1] // head_count
        )

    block_query = to_blocks(queries)
    block_key = to_blocks(keys_all)
    block_value = to_blocks(values_all)
    cumulative = jnp.cumsum(to_blocks(decay_logarithm), axis=1)
    middle = cumulative[:, halfway - 1 : halfway]
    query_local = block_query * jnp.exp(cumulative - middle)
    key_local = block_key * jnp.exp(middle - cumulative)
    scores = jnp.einsum("nthd,nshd->nhts", query_local, key_local, precision=highest)
    scores = jnp.where(causal[None, None], scores, 0.0)
    within = jnp.einsum("nhts,nshv->nthv", scores, block_value, precision=highest)
    lasting = cumulative[:, -1]
    update = jnp.einsum(
        "nshd,nshv->nhdv",
        block_key * jnp.exp(lasting[:, None] - cumulative),
        block_value,
        precision=highest,
    )

    def advance(memory, inputs):
        fade, addition = inputs
        return (jnp.exp(fade)[:, :, None] * memory + addition, memory)

    key_width = queries.shape[1] // head_count
    value_width = values_all.shape[1] // head_count
    initial = jnp.zeros((head_count, key_width, value_width), jnp.float32)
    earlier = lax.scan(advance, initial, (lasting, update))[1]
    carried = jnp.einsum(
        "nthd,nhdv->nthv", block_query * jnp.exp(cumulative), earlier, precision=highest
    )
    return (within + carried).reshape(length, head_count, value_width)


def project_inputs(source, weight):
    return jnp.dot(source, weight, preferred_element_type=jnp.float32)


def local(
    activations,
    mixer_gain,
    query_weight,
    key_weight,
    value_weight,
    rank_weight,
    decay_gate_weight,
    decay_gate_bias,
    head_gain,
    output_weight,
    ffn_gain,
    gate_weight,
    up_weight,
    down_weight,
):
    residual = activations.astype(jnp.float32)
    normed = rms_scale(residual, mixer_gain).astype(jnp.bfloat16)
    rank_slice = project_inputs(normed, rank_weight).astype(jnp.bfloat16)
    sequence, rank_slices_gathered = (
        lax.all_gather(normed, "tp", axis=0, tiled=True),
        lax.all_gather(rank_slice, "tp", axis=0, tiled=True),
    )
    length = sequence.shape[0]
    query_full, key_full, value_full = (
        lax.all_gather(query_weight, "fs", axis=0, tiled=True),
        lax.all_gather(key_weight, "fs", axis=0, tiled=True),
        lax.all_gather(value_weight, "fs", axis=0, tiled=True),
    )
    queries = project_inputs(sequence, query_full).astype(jnp.bfloat16)
    keys_all = project_inputs(sequence, key_full).astype(jnp.bfloat16)
    values_all = project_inputs(sequence, value_full).astype(jnp.bfloat16)
    decay_logarithm = (
        jax.nn.log_sigmoid(
            project_inputs(rank_slices_gathered, decay_gate_weight) + decay_gate_bias
        )
        / decay_softness
    )
    head_count = query_weight.shape[1] // DK
    attended = linear_attention(queries, keys_all, values_all, decay_logarithm, head_count)
    head_rows = rms_scale(attended, head_gain).astype(jnp.bfloat16).reshape(length, head_count * DV)
    own_rows = lax.all_to_all(head_rows, "tp", split_axis=0, concat_axis=1, tiled=True)
    tall_out = lax.all_gather(output_weight, "tp", axis=0, tiled=True)
    whole_out = lax.all_gather(tall_out, "fs", axis=1, tiled=True)
    mixed = residual + project_inputs(own_rows, whole_out)
    ffn_normed = rms_scale(mixed, ffn_gain).astype(jnp.bfloat16)
    ffn_sequence = lax.all_gather(ffn_normed, "tp", axis=0, tiled=True)
    gate_full, up_full = (
        lax.all_gather(gate_weight, "fs", axis=0, tiled=True),
        lax.all_gather(up_weight, "fs", axis=0, tiled=True),
    )
    down_full = lax.all_gather(down_weight, "fs", axis=1, tiled=True)
    hidden = (
        jax.nn.silu(project_inputs(ffn_sequence, gate_full)) * project_inputs(ffn_sequence, up_full)
    ).astype(jnp.bfloat16)
    result = mixed + lax.psum_scatter(
        project_inputs(hidden, down_full).astype(jnp.bfloat16),
        "tp",
        scatter_dimension=0,
        tiled=True,
    ).astype(jnp.float32)
    return result.astype(jnp.bfloat16)


def solution(mesh):
    in_specs = (
        P(("rep", "fs", "tp"), None),
        P(),
        P("fs", "tp"),
        P("fs", "tp"),
        P("fs", "tp"),
        P(),
        P(None, "tp"),
        P("tp"),
        P(),
        P("tp", "fs"),
        P(),
        P("fs", "tp"),
        P("fs", "tp"),
        P("tp", "fs"),
    )
    out_specs = P(("rep", "fs", "tp"), None)
    return jax.shard_map(local, mesh=mesh, in_specs=in_specs, out_specs=out_specs, check_vma=False)
```

profile of v0, /device:TPU:0, one launch (start us, length us, event | category | flops | bytes accessed | tf_op | source)
XLA Modules:
  0.0 369.9 jit_solution(17549334003282702146)
XLA Ops:
  6.5 1.5 fusion.2
  8.1 2.5 fusion.4
  10.7 2.2 all_gather.38
  13.0 1.6 convolution_convert_fusion.3
  14.6 2.1 all_gather.36
  16.8 0.5 fusion.12
  17.2 0.3 fusion.24
  17.6 32.6 %all_gather.37 = bf16[1024,128]{1,0:T(8,128)(2,1)S(1)} all-gather(bf16[128,128]{1,0:T(8,128)(2,1)S(1)} %copy-done.8), channel_id=1, replica_groups=mesh['rep'=2,'fs'=8,'tp'=2] {'fs'}, dimensions={0}, use_global_device_ids=true | all-gather | bytes 294912 | tf_op jit(solution)/shard_map/all_gather | solution.py:91
  50.2 31.1 %all_gather.35 = bf16[1024,128]{1,0:T(8,128)(2,1)S(1)} all-gather(bf16[128,128]{1,0:T(8,128)(2,1)S(1)} %copy-done.9), channel_id=1, replica_groups=mesh['rep'=2,'fs'=8,'tp'=2] {'fs'}, dimensions={0}, use_global_device_ids=true | all-gather | bytes 294912 | tf_op jit(solution)/shard_map/all_gather | solution.py:90
  81.3 31.3 %all_gather.34 = bf16[1024,256]{1,0:T(8,128)(2,1)S(1)} all-gather(bf16[128,256]{1,0:T(8,128)(2,1)S(1)} %copy-done.7), channel_id=1, replica_groups=mesh['rep'=2,'fs'=8,'tp'=2] {'fs'}, dimensions={0}, use_global_device_ids=true | all-gather | bytes 589824 | tf_op jit(solution)/shard_map/all_gather | solution.py:92
  112.6 2.4 convolution_convert_fusion.1
  115.1 0.7 convolution_convert_fusion.2
  115.8 1.6 fusion.14
  117.4 0.7 convolution_convert_fusion
  118.1 1.1 convolution_bitcast_fusion
  119.2 12.6 %while.13 = (s32[]{:T(128)}, f32[1,128,256]{2,1,0:T(8,128)S(1)}, f32[16,1,128,256]{3,2,1,0:T(8,128)}, f32[16,1,128]{2,1,0:T(1,128)S(1)}, f32[16,1,128,256]{3,2,1,0:T(8,128)S(1)}, /*index=5*/s32[]{:T(128)}, s32[]{:T(128)}) while((s32[]{:T(128)}, f32[1,128,256]{2,1,0:T(8,128)S(1)}, f32[16,1,128,256]{3,2,1,0:T(8,128)}, ...), condition=%wide.region_3.4_spmd.clone, body=%wide.region_2.3_spmd.clone.sunk | while | flops 131075 | bytes 657504 | solution.py:54
  119.2 0.7 bitcast_dynamic-update-slice_fusion.2
  119.9 0.1 bitcast_add_fusion.2
  120.0 0.7 bitcast_dynamic-update-slice_fusion.2
  120.7 0.1 bitcast_add_fusion.2
  120.8 0.7 bitcast_dynamic-update-slice_fusion.2
  121.4 0.1 bitcast_add_fusion.2
  121.6 0.7 bitcast_dynamic-update-slice_fusion.2
  122.2 0.1 bitcast_add_fusion.2
  122.3 0.7 bitcast_dynamic-update-slice_fusion.2
  123.0 0.1 bitcast_add_fusion.2
  123.1 0.7 bitcast_dynamic-update-slice_fusion.2
  123.8 0.1 bitcast_add_fusion.2
  123.9 0.6 bitcast_dynamic-update-slice_fusion.2
  124.6 0.1 bitcast_add_fusion.2
  124.7 0.7 bitcast_dynamic-update-slice_fusion.2
  125.4 0.1 bitcast_add_fusion.2
  125.5 0.7 bitcast_dynamic-update-slice_fusion.2
  126.2 0.1 bitcast_add_fusion.2
  126.3 0.7 bitcast_dynamic-update-slice_fusion.2
  127.1 0.7 bitcast_dynamic-update-slice_fusion.2
  127.7 0.1 bitcast_add_fusion.2
  127.9 0.7 bitcast_dynamic-update-slice_fusion.2
  128.7 0.7 bitcast_dynamic-update-slice_fusion.2
  129.4 0.7 bitcast_dynamic-update-slice_fusion.2
  130.2 0.7 bitcast_dynamic-update-slice_fusion.2
  131.0 0.7 bitcast_dynamic-update-slice_fusion.2
  131.8 2.2 convolution_select_fusion
  134.1 3.0 fusion.5
  137.1 0.7 fusion.10
  137.8 0.3 copy.33
  138.3 0.9 multiply_convert_fusion.2
  139.2 3.5 all-to-all-start
  142.8 1.7 all-to-all-done
  144.4 0.8 copy-done.3
  145.2 2.2 multiply_reduce_fusion
  147.5 1.2 multiply_convert_fusion.1
  148.7 0.5 all-gather.13.cloned.1.call-update
  149.3 0.5 all-gather.15.cloned.1.call-update
  149.9 0.5 all-gather.17.cloned.1.call-update
  150.4 0.2 reduce-scatter.2.cloned.1.call-start
  150.7 10.0 %all-gather.11.cloned.1.call-done = bf16[1024,1024]{1,0:T(8,128)(2,1)} async-done(((bf16[512,1024]{1,0:T(8,128)(2,1)}), bf16[1024,1024]{1,0:T(8,128)(2,1)}) %all-gather.11.cloned.1.call-update) | async-done | bytes 2097168 | tf_op jit(solution)/shard_map/all_gather | solution.py:111
  160.7 60.5 %all-gather.13.cloned.1.call-done = bf16[1024,1408]{1,0:T(8,128)(2,1)} async-done(((bf16[128,1408]{1,0:T(8,128)(2,1)}), bf16[1024,1408]{1,0:T(8,128)(2,1)}) %all-gather.13.cloned.1.call-update) | async-done | bytes 2883600 | tf_op jit(solution)/shard_map/all_gather | solution.py:113
  221.2 8.3 %fusion.27 = f32[1024,1408]{1,0:T(8,128)} fusion(bf16[1024,1024]{1,0:T(8,128)(2,1)} %all-gather.11.cloned.1.call-done, bf16[1024,1408]{1,0:T(8,128)(2,1)} %all-gather.13.cloned.1.call-done), kind=kOutput, calls=%fused_computation.58 | convolution fusion | flops 2952790016 | bytes 10747904 | tf_op jit(solution)/shard_map/dot_general | solution.py:62
  229.6 49.6 %all-gather.15.cloned.1.call-done = bf16[1024,1408]{1,0:T(8,128)(2,1)} async-done(((bf16[128,1408]{1,0:T(8,128)(2,1)}), bf16[1024,1408]{1,0:T(8,128)(2,1)}) %all-gather.15.cloned.1.call-update) | async-done | bytes 2883600 | tf_op jit(solution)/shard_map/all_gather | solution.py:114
  279.2 60.1 %all-gather.17.cloned.1.call-done = bf16[1408,1024]{1,0:T(8,128)(2,1)} async-done(((bf16[1408,128]{1,0:T(8,128)(2,1)}), bf16[1408,1024]{1,0:T(8,128)(2,1)}) %all-gather.17.cloned.1.call-update) | async-done | bytes 2883600 | tf_op jit(solution)/shard_map/all_gather | solution.py:116
  339.3 13.1 %fusion.8 = bf16[1024,1024]{1,0:T(8,128)(2,1)} fusion(bf16[1408,1024]{1,0:T(8,128)(2,1)} %all-gather.17.cloned.1.call-done, f32[1024,1408]{1,0:T(8,128)} %fusion.27, bf16[1024,1024]{1,0:T(8,128)(2,1)} %all-gather.11.cloned.1.call-done, bf16[1024,1408]{1,0:T(8,128)(2,1)} %all-gather.15.cloned.1.call-done), kind=kOutput, calls=%fused_computation.18 | convolution fusion | flops 5915279360 | bytes 15728640 | tf_op jit(solution)/shard_map/dot_general | solution.py:62
  352.4 8.1 %reduce-scatter.2.cloned.1.call-done = bf16[512,1024]{1,0:T(8,128)(2,1)} async-done(((bf16[1024,1024]{1,0:T(8,128)(2,1)}), bf16[512,1024]{1,0:T(8,128)(2,1)}) %reduce-scatter.2.cloned.1.call-update) | async-done | bytes 1048592 | tf_op jit(solution)/shard_map/reduce_scatter | solution.py:120
  360.5 2.5 add_convert_fusion
  (71 shorter events, 1.2 us)
Async XLA Ops:
  6.5 6.4 %copy-start = (bf16[1024,16]{0,1:T(8,128)(2,1)S(1)}, bf16[1024,16]{0,1:T(8,128)(2,1)}, u32[]{:S(2)}) copy-start(bf16[1024,16]{0,1:T(8,128)(2,1)} %param.21) | copy-start | bytes 98308
  6.5 106.0 %all-gather.7.cloned.1.call-start = ((), (), s32[]{:S(2)}) async-start(), calls=%async_computation.2 | async-start | bytes 3145728 | tf_op jit(solution)/shard_map/all_gather | solution.py:85
  6.5 4.2 %copy-start.6 = (bf16[256,128]{1,0:T(8,128)(2,1)S(1)}, bf16[256,128]{1,0:T(8,128)(2,1)}, u32[]{:S(2)}) copy-start(bf16[256,128]{1,0:T(8,128)(2,1)} %param.25) | copy-start | bytes 196612
  8.1 8.7 %copy-start.12 = (bf16[16,128]{1,0:T(8,128)(2,1)S(1)}, bf16[16,128]{1,0:T(8,128)(2,1)}, u32[]{:S(2)}) copy-start(bf16[16,128]{1,0:T(8,128)(2,1)} %param.22) | copy-start | bytes 12292
  8.1 8.7 %copy-start.13 = (f32[128]{0:T(128)S(1)}, f32[128]{0:T(128)}, u32[]{:S(2)}) copy-start(f32[128]{0:T(128)} %param.23) | copy-start | bytes 1540
  10.7 132.1 %all-gather.9.cloned.1.call-start = ((), (), s32[]{:S(2)}) async-start(), calls=%async_computation.3 | async-start | bytes 1179648 | tf_op jit(solution)/shard_map/all_gather | solution.py:108
  13.0 4.6 %copy-start.8 = (bf16[128,128]{1,0:T(8,128)(2,1)S(1)}, bf16[128,128]{1,0:T(8,128)(2,1)}, u32[]{:S(2)}) copy-start(bf16[128,128]{1,0:T(8,128)(2,1)} %param.19) | copy-start | bytes 98308
  14.6 35.6 %copy-start.9 = (bf16[128,128]{1,0:T(8,128)(2,1)S(1)}, bf16[128,128]{1,0:T(8,128)(2,1)}, u32[]{:S(2)}) copy-start(bf16[128,128]{1,0:T(8,128)(2,1)} %param.18) | copy-start | bytes 98308
  14.6 66.6 %copy-start.7 = (bf16[128,256]{1,0:T(8,128)(2,1)S(1)}, bf16[128,256]{1,0:T(8,128)(2,1)}, u32[]{:S(2)}) copy-start(bf16[128,256]{1,0:T(8,128)(2,1)} %param.20) | copy-start | bytes 196612
  112.6 2.5 copy-start.2
  118.1 1.1 copy-start.4
  134.0 3.0 copy-start.5
  137.1 1.2 copy-start.11
  137.8 7.4 %copy-start.1 = (bf16[512,1024]{1,0:T(8,128)(2,1)S(1)}, bf16[512,1024]{1,0:T(8,128)(2,1)}, u32[]{:S(2)}) copy-start(bf16[512,1024]{1,0:T(8,128)(2,1)} %param.16) | copy-start | bytes 3145732
  139.2 5.2 %all-to-all-start = ((bf16[2,512,256]{1,2,0:T(8,128)(2,1)}), bf16[2,512,256]{1,2,0:T(8,128)(2,1)S(1)}, u32[]{:S(2)}, u32[]{:S(2)}) async-start(bf16[2,512,256]{1,2,0:T(8,128)(2,1)} %multiply_convert_fusion.2), calls=%async_computation | async-start | bytes 1048576 | tf_op jit(solution)/shard_map/all_to_all | solution.py:106
  142.7 18.0 %all-gather.11.cloned.1.call-start = ((), (), s32[]{:S(2)}) async-start(), calls=%async_computation.4 | async-start | bytes 3145728 | tf_op jit(solution)/shard_map/all_gather | solution.py:111
  144.4 0.8 copy-start.3
  145.2 2.2 copy-start.10
  148.7 72.5 %all-gather.13.cloned.1.call-start = ((), (), s32[]{:S(2)}) async-start(), calls=%async_computation.5 | async-start | bytes 3244032 | tf_op jit(solution)/shard_map/all_gather | solution.py:113
  149.3 129.9 %all-gather.15.cloned.1.call-start = ((), (), s32[]{:S(2)}) async-start(), calls=%async_computation.6 | async-start | bytes 3244032 | tf_op jit(solution)/shard_map/all_gather | solution.py:114
  149.9 189.5 %all-gather.17.cloned.1.call-start = ((), (), s32[]{:S(2)}) async-start(), calls=%async_computation.7 | async-start | bytes 3244032 | tf_op jit(solution)/shard_map/all_gather | solution.py:116
  150.4 210.1 %reduce-scatter.2.cloned.1.call-start = ((), (), s32[]{:S(2)}) async-start(), calls=%async_computation.8 | async-start | bytes 3145728 | tf_op jit(solution)/shard_map/reduce_scatter | solution.py:120
Sparse Core Ops, SparseCore 0:
  10.8 13.2 all-gather.6
  26.1 42.2 all-gather.8
  148.8 11.8 all-gather.10
  162.7 58.4 all-gather.12
  223.3 55.9 all-gather.14
  281.1 58.1 all-gather.16
  352.5 7.9 reduce-scatter.1
where the time goes:
time: 370 us
  waiting for transfers between devices  192 us (52%)
  blocking collectives  99.3 us (27%)
  matrix products  36.6 us (10%)
  other arithmetic  22.9 us (6%)
  between operations  13.8 us (4%)
  starting transfers between devices  3.91 us (1%)
    all_gather x1, waiting for transfers between devices, local(): lax.all_gather(gate_weight, 'fs', axis=0, tiled=True)  60.5 us
    all_gather x1, waiting for transfers between devices, local(): down_full = lax.all_gather(down_weight, 'fs', axis=1, tiled=True)  60.1 us
    all_gather x1, waiting for transfers between devices, local(): lax.all_gather(up_weight, 'fs', axis=0, tiled=True)  49.6 us
    all_gather x1, blocking collectives, local(): lax.all_gather(key_weight, 'fs', axis=0, tiled=True)  32.6 us
    all_gather x1, blocking collectives, local(): lax.all_gather(value_weight, 'fs', axis=0, tiled=True)  31.3 us
    all_gather x1, blocking collectives, local(): lax.all_gather(query_weight, 'fs', axis=0, tiled=True)  31.1 us
    dot_general x8, matrix products, project_inputs(): return jnp.dot(source, weight, preferred_element_type=jnp.float32)  29.6 us
    dynamic_update_slice x16, other arithmetic, linear_attention(): earlier = lax.scan(advance, initial, (lasting, update))[1]  10.6 us
  transfers between devices with their start and end apart: 8, of which 6 were waited for; matrix products, arithmetic and copies ran while one was open for 10% of the time, Pallas kernels for 0%

commit v1 on v0

--- a/solution.py
+++ b/solution.py
@@ -87,7 +87,15 @@
     )
     length = sequence.shape[0]
     query_full, key_full, value_full = (
-        lax.all_gather(query_weight, "fs", axis=0, tiled=True),
+        jnp.concatenate(
+            lax.all_to_all(
+                jnp.stack([query_weight] * lax.psum(1, axis_name="fs")),
+                axis_name="fs",
+                split_axis=0,
+                concat_axis=0,
+            ),
+            axis=0,
+        ),
         lax.all_gather(key_weight, "fs", axis=0, tiled=True),
         lax.all_gather(value_weight, "fs", axis=0, tiled=True),
     )

time: 370 us -> 346 us (0.935)
  blocking collectives: 99.3 us -> 67.8 us
  starting transfers between devices: 3.91 us -> 11.2 us
    all_gather x1 -> x0, blocking collectives: 31.1 us -> none  [local(): lax.all_gather(query_weight, 'fs', axis=0, tiled=True)]
    all_to_all x0 -> x1, starting transfers between devices: none -> 7.31 us  [local(): lax.all_to_all(jnp.stack([query_weight] * lax.psum(1, axis_name='fs')), a...]
  transfers between devices with their start and end apart: 8 -> 9, of which waited for: 6 -> 6; matrix products, arithmetic and copies ran while one was open for 10% -> 11% of each run, Pallas kernels for 0% -> 0%
where the time goes in v1:
time: 346 us; the launch traced here: 345 us
  waiting for transfers between devices  192 us (55%)
  blocking collectives  67.8 us (20%)
  matrix products  35.4 us (10%)
  other arithmetic  23 us (7%)
  between operations  13.8 us (4%)
  starting transfers between devices  11.2 us (3%)
    all_gather x1, waiting for transfers between devices, local(): lax.all_gather(gate_weight, 'fs', axis=0, tiled=True)  60.5 us
    all_gather x1, waiting for transfers between devices, local(): down_full = lax.all_gather(down_weight, 'fs', axis=1, tiled=True)  60.1 us
    all_gather x1, waiting for transfers between devices, local(): lax.all_gather(up_weight, 'fs', axis=0, tiled=True)  49.6 us
    all_gather x1, blocking collectives, local(): lax.all_gather(value_weight, 'fs', axis=0, tiled=True)  31.9 us
    all_gather x1, blocking collectives, local(): lax.all_gather(key_weight, 'fs', axis=0, tiled=True)  31.5 us
    dot_general x8, matrix products, project_inputs(): return jnp.dot(source, weight, preferred_element_type=jnp.float32)  28.3 us
    dynamic_update_slice x16, other arithmetic, linear_attention(): earlier = lax.scan(advance, initial, (lasting, update))[1]  10.6 us
    all_gather x1, waiting for transfers between devices, local(): ffn_sequence = lax.all_gather(ffn_normed, 'tp', axis=0, tiled=True)  9.87 us
  transfers between devices with their start and end apart: 9, of which 6 were waited for; matrix products, arithmetic and copies ran while one was open for 11% of the time, Pallas kernels for 0%

profile of v1, /device:TPU:0, one launch (start us, length us, event | category | flops | bytes accessed | tf_op | source)
XLA Modules:
  0.0 345.2 jit_solution(13370195524275406262)
XLA Ops:
  6.5 1.5 fusion.2
  8.1 2.5 fusion.4
  10.7 0.7 stack.2
  11.4 7.3 %all-to-all-start = ((bf16[8,128,128]{2,1,0:T(8,128)(2,1)}), bf16[8,128,128]{2,1,0:T(8,128)(2,1)S(1)}, u32[]{:S(2)}, u32[]{:S(2)}) async-start(bf16[8,128,128]{2,1,0:T(8,128)(2,1)} %stack.2), calls=%async_computation | async-start | bytes 524288 | tf_op jit(solution)/shard_map/all_to_all | solution.py:91
  18.8 2.0 all_gather.34
  20.9 0.4 convolution_convert_fusion.3
  21.3 2.3 all_gather.32
  23.6 0.5 fusion.12
  24.1 0.3 fusion.24
  24.4 31.5 %all_gather.33 = bf16[1024,128]{1,0:T(8,128)(2,1)S(1)} all-gather(bf16[128,128]{1,0:T(8,128)(2,1)S(1)} %copy-done.10), channel_id=1, replica_groups=mesh['rep'=2,'fs'=8,'tp'=2] {'fs'}, dimensions={0}, use_global_device_ids=true | all-gather | bytes 294912 | tf_op jit(solution)/shard_map/all_gather | solution.py:99
  56.0 31.9 %all_gather.31 = bf16[1024,256]{1,0:T(8,128)(2,1)S(1)} all-gather(bf16[128,256]{1,0:T(8,128)(2,1)S(1)} %copy-done.8), channel_id=1, replica_groups=mesh['rep'=2,'fs'=8,'tp'=2] {'fs'}, dimensions={0}, use_global_device_ids=true | all-gather | bytes 589824 | tf_op jit(solution)/shard_map/all_gather | solution.py:100
  87.9 2.4 convolution_convert_fusion.2
  90.4 0.7 convolution_convert_fusion.1
  91.1 1.6 fusion.14
  92.7 0.7 convolution_convert_fusion
  93.4 1.1 convolution_bitcast_fusion
  94.5 12.7 %while.13 = (s32[]{:T(128)}, f32[1,128,256]{2,1,0:T(8,128)S(1)}, f32[16,1,128,256]{3,2,1,0:T(8,128)}, f32[16,1,128]{2,1,0:T(1,128)S(1)}, f32[16,1,128,256]{3,2,1,0:T(8,128)S(1)}, /*index=5*/s32[]{:T(128)}, s32[]{:T(128)}) while((s32[]{:T(128)}, f32[1,128,256]{2,1,0:T(8,128)S(1)}, f32[16,1,128,256]{3,2,1,0:T(8,128)}, ...), condition=%wide.region_3.4_spmd.clone, body=%wide.region_2.3_spmd.clone.sunk | while | flops 131075 | bytes 657504 | solution.py:54
  94.5 0.7 bitcast_dynamic-update-slice_fusion.2
  95.3 0.7 bitcast_dynamic-update-slice_fusion.2
  96.0 0.1 bitcast_add_fusion.2
  96.1 0.7 bitcast_dynamic-update-slice_fusion.2
  96.8 0.1 bitcast_add_fusion.2
  96.9 0.7 bitcast_dynamic-update-slice_fusion.2
  97.6 0.1 bitcast_add_fusion.2
  97.7 0.7 bitcast_dynamic-update-slice_fusion.2
  98.4 0.1 bitcast_add_fusion.2
  98.5 0.7 bitcast_dynamic-update-slice_fusion.2
  99.2 0.1 bitcast_add_fusion.2
  99.3 0.7 bitcast_dynamic-update-slice_fusion.2
  100.0 0.1 bitcast_add_fusion.2
  100.1 0.7 bitcast_dynamic-update-slice_fusion.2
  100.9 0.7 bitcast_dynamic-update-slice_fusion.2
  101.5 0.1 bitcast_add_fusion.2
  101.7 0.7 bitcast_dynamic-update-slice_fusion.2
  102.4 0.7 bitcast_dynamic-update-slice_fusion.2
  103.1 0.1 bitcast_add_fusion.2
  103.2 0.7 bitcast_dynamic-update-slice_fusion.2
  103.9 0.1 bitcast_add_fusion.2
  104.0 0.7 bitcast_dynamic-update-slice_fusion.2
  104.8 0.7 bitcast_dynamic-update-slice_fusion.2
  105.6 0.7 bitcast_dynamic-update-slice_fusion.2
  106.4 0.7 bitcast_dynamic-update-slice_fusion.2
  107.2 2.2 convolution_select_fusion
  109.5 3.0 fusion.5
  112.5 0.7 fusion.10
  113.2 0.3 copy.33
  113.7 0.9 multiply_convert_fusion.2
  114.6 3.5 %all-to-all-start.1 = ((bf16[2,512,256]{1,2,0:T(8,128)(2,1)}), bf16[2,512,256]{1,2,0:T(8,128)(2,1)S(1)}, u32[]{:S(2)}, u32[]{:S(2)}) async-start(bf16[2,512,256]{1,2,0:T(8,128)(2,1)} %multiply_convert_fusion.2), calls=%async_computation.1 | async-start | bytes 1048576 | tf_op jit(solution)/shard_map/all_to_all | solution.py:114
  118.2 1.7 all-to-all-done.1
  119.8 0.8 copy-done.4
  120.6 2.2 multiply_reduce_fusion
  122.9 1.2 multiply_convert_fusion.1
  124.2 0.5 all-gather.13.cloned.1.call-update
  124.7 0.5 all-gather.15.cloned.1.call-update
  125.3 0.5 all-gather.17.cloned.1.call-update
  125.8 0.2 reduce-scatter.2.cloned.1.call-start
  126.1 9.9 %all-gather.11.cloned.1.call-done = bf16[1024,1024]{1,0:T(8,128)(2,1)} async-done(((bf16[512,1024]{1,0:T(8,128)(2,1)}), bf16[1024,1024]{1,0:T(8,128)(2,1)}) %all-gather.11.cloned.1.call-update) | async-done | bytes 2097168 | tf_op jit(solution)/shard_map/all_gather | solution.py:119
  135.9 60.5 %all-gather.13.cloned.1.call-done = bf16[1024,1408]{1,0:T(8,128)(2,1)} async-done(((bf16[128,1408]{1,0:T(8,128)(2,1)}), bf16[1024,1408]{1,0:T(8,128)(2,1)}) %all-gather.13.cloned.1.call-update) | async-done | bytes 2883600 | tf_op jit(solution)/shard_map/all_gather | solution.py:121
  196.5 8.3 %fusion.27 = f32[1024,1408]{1,0:T(8,128)} fusion(bf16[1024,1024]{1,0:T(8,128)(2,1)} %all-gather.11.cloned.1.call-done, bf16[1024,1408]{1,0:T(8,128)(2,1)} %all-gather.13.cloned.1.call-done), kind=kOutput, calls=%fused_computation.58 | convolution fusion | flops 2952790016 | bytes 10747904 | tf_op jit(solution)/shard_map/dot_general | solution.py:62
  204.8 49.6 %all-gather.15.cloned.1.call-done = bf16[1024,1408]{1,0:T(8,128)(2,1)} async-done(((bf16[128,1408]{1,0:T(8,128)(2,1)}), bf16[1024,1408]{1,0:T(8,128)(2,1)}) %all-gather.15.cloned.1.call-update) | async-done | bytes 2883600 | tf_op jit(solution)/shard_map/all_gather | solution.py:122
  254.5 60.1 %all-gather.17.cloned.1.call-done = bf16[1408,1024]{1,0:T(8,128)(2,1)} async-done(((bf16[1408,128]{1,0:T(8,128)(2,1)}), bf16[1408,1024]{1,0:T(8,128)(2,1)}) %all-gather.17.cloned.1.call-update) | async-done | bytes 2883600 | tf_op jit(solution)/shard_map/all_gather | solution.py:124
  314.6 13.0 %fusion.8 = bf16[1024,1024]{1,0:T(8,128)(2,1)} fusion(bf16[1408,1024]{1,0:T(8,128)(2,1)} %all-gather.17.cloned.1.call-done, f32[1024,1408]{1,0:T(8,128)} %fusion.27, bf16[1024,1024]{1,0:T(8,128)(2,1)} %all-gather.11.cloned.1.call-done, bf16[1024,1408]{1,0:T(8,128)(2,1)} %all-gather.15.cloned.1.call-done), kind=kOutput, calls=%fused_computation.18 | convolution fusion | flops 5915279360 | bytes 15728640 | tf_op jit(solution)/shard_map/dot_general | solution.py:62
  327.7 8.1 %reduce-scatter.2.cloned.1.call-done = bf16[512,1024]{1,0:T(8,128)(2,1)} async-done(((bf16[1024,1024]{1,0:T(8,128)(2,1)}), bf16[512,1024]{1,0:T(8,128)(2,1)}) %reduce-scatter.2.cloned.1.call-update) | async-done | bytes 1048592 | tf_op jit(solution)/shard_map/reduce_scatter | solution.py:128
  335.8 2.5 add_convert_fusion
  (75 shorter events, 1.3 us)
Async XLA Ops:
  6.5 14.3 %copy-start = (bf16[1024,16]{0,1:T(8,128)(2,1)S(1)}, bf16[1024,16]{0,1:T(8,128)(2,1)}, u32[]{:S(2)}) copy-start(bf16[1024,16]{0,1:T(8,128)(2,1)} %param.21) | copy-start | bytes 98308
  6.5 81.3 %all-gather.7.cloned.1.call-start = ((), (), s32[]{:S(2)}) async-start(), calls=%async_computation.3 | async-start | bytes 3145728 | tf_op jit(solution)/shard_map/all_gather | solution.py:85
  6.5 4.1 %copy-start.9 = (bf16[128,128]{1,0:T(8,128)(2,1)S(1)}, bf16[128,128]{1,0:T(8,128)(2,1)}, u32[]{:S(2)}) copy-start(bf16[128,128]{1,0:T(8,128)(2,1)} %param.18) | copy-start | bytes 98308
  8.1 10.7 %copy-start.7 = (bf16[256,128]{1,0:T(8,128)(2,1)S(1)}, bf16[256,128]{1,0:T(8,128)(2,1)}, u32[]{:S(2)}) copy-start(bf16[256,128]{1,0:T(8,128)(2,1)} %param.25) | copy-start | bytes 196612
  10.6 10.2 %copy-start.3 = (bf16[512,1024]{1,0:T(8,128)(2,1)S(1)}, bf16[512,1024]{1,0:T(8,128)(2,1)}, u32[]{:S(2)}) copy-start(bf16[512,1024]{1,0:T(8,128)(2,1)} %fusion.4) | copy-start | bytes 3145732
  10.6 13.0 %copy-start.13 = (bf16[16,128]{1,0:T(8,128)(2,1)S(1)}, bf16[16,128]{1,0:T(8,128)(2,1)}, u32[]{:S(2)}) copy-start(bf16[16,128]{1,0:T(8,128)(2,1)} %param.22) | copy-start | bytes 12292
  10.6 13.0 %copy-start.14 = (f32[128]{0:T(128)S(1)}, f32[128]{0:T(128)}, u32[]{:S(2)}) copy-start(f32[128]{0:T(128)} %param.23) | copy-start | bytes 1540
  11.4 76.5 %all-to-all-start = ((bf16[8,128,128]{2,1,0:T(8,128)(2,1)}), bf16[8,128,128]{2,1,0:T(8,128)(2,1)S(1)}, u32[]{:S(2)}, u32[]{:S(2)}) async-start(bf16[8,128,128]{2,1,0:T(8,128)(2,1)} %stack.2), calls=%async_computation | async-start | bytes 524288 | tf_op jit(solution)/shard_map/all_to_all | solution.py:91
  18.7 99.5 %all-gather.9.cloned.1.call-start = ((), (), s32[]{:S(2)}) async-start(), calls=%async_computation.4 | async-start | bytes 1179648 | tf_op jit(solution)/shard_map/all_gather | solution.py:116
  20.9 3.5 %copy-start.10 = (bf16[128,128]{1,0:T(8,128)(2,1)S(1)}, bf16[128,128]{1,0:T(8,128)(2,1)}, u32[]{:S(2)}) copy-start(bf16[128,128]{1,0:T(8,128)(2,1)} %param.19) | copy-start | bytes 98308
  21.3 34.7 %copy-start.8 = (bf16[128,256]{1,0:T(8,128)(2,1)S(1)}, bf16[128,256]{1,0:T(8,128)(2,1)}, u32[]{:S(2)}) copy-start(bf16[128,256]{1,0:T(8,128)(2,1)} %param.20) | copy-start | bytes 196612
  87.9 2.5 copy-start.2
  93.4 1.1 copy-start.5
  109.5 3.0 copy-start.6
  112.5 1.2 copy-start.12
  113.2 7.4 %copy-start.1 = (bf16[512,1024]{1,0:T(8,128)(2,1)S(1)}, bf16[512,1024]{1,0:T(8,128)(2,1)}, u32[]{:S(2)}) copy-start(bf16[512,1024]{1,0:T(8,128)(2,1)} %param.16) | copy-start | bytes 3145732
  114.6 5.2 %all-to-all-start.1 = ((bf16[2,512,256]{1,2,0:T(8,128)(2,1)}), bf16[2,512,256]{1,2,0:T(8,128)(2,1)S(1)}, u32[]{:S(2)}, u32[]{:S(2)}) async-start(bf16[2,512,256]{1,2,0:T(8,128)(2,1)} %multiply_convert_fusion.2), calls=%async_computation.1 | async-start | bytes 1048576 | tf_op jit(solution)/shard_map/all_to_all | solution.py:114
  118.1 17.8 %all-gather.11.cloned.1.call-start = ((), (), s32[]{:S(2)}) async-start(), calls=%async_computation.5 | async-start | bytes 3145728 | tf_op jit(solution)/shard_map/all_gather | solution.py:119
  119.8 0.8 copy-start.4
  120.6 2.2 copy-start.11
  124.1 72.4 %all-gather.13.cloned.1.call-start = ((), (), s32[]{:S(2)}) async-start(), calls=%async_computation.6 | async-start | bytes 3244032 | tf_op jit(solution)/shard_map/all_gather | solution.py:121
  124.7 129.8 %all-gather.15.cloned.1.call-start = ((), (), s32[]{:S(2)}) async-start(), calls=%async_computation.7 | async-start | bytes 3244032 | tf_op jit(solution)/shard_map/all_gather | solution.py:122
  125.3 189.3 %all-gather.17.cloned.1.call-start = ((), (), s32[]{:S(2)}) async-start(), calls=%async_computation.8 | async-start | bytes 3244032 | tf_op jit(solution)/shard_map/all_gather | solution.py:124
  125.8 209.9 %reduce-scatter.2.cloned.1.call-start = ((), (), s32[]{:S(2)}) async-start(), calls=%async_computation.9 | async-start | bytes 3145728 | tf_op jit(solution)/shard_map/reduce_scatter | solution.py:128
Sparse Core Ops, SparseCore 0:
  10.8 13.4 all-gather.6
  26.3 43.2 all-gather.8
  124.2 11.6 all-gather.10
  138.0 58.4 all-gather.12
  198.5 55.9 all-gather.14
  256.4 58.1 all-gather.16
  327.8 7.9 reduce-scatter.1
